TPU v7x, 32 devices: a whole 2x2x4 slice. The times are simulated.
32 devices in a mesh: fs: 8 (over z, y), tp: 4 (over x, core).
Axes of the slice: x: 2, y: 2, z: 4, core: 2. Of those that a mesh axis runs over, the one named last changes fastest.
Arguments:
- saved_input: bfloat16 [16384, 2048], P('fs'), may hold values from -6 to 6
- query_cotangent: bfloat16 [16384, 2048], P('fs', 'tp'), may hold values from -0.046875 to 0.046875
- forget_cotangent: bfloat16 [16384, 2048], P('fs', 'tp'), may hold values from -0.046875 to 0.046875
- mixed_output: bfloat16 [16384, 2048], P('fs', 'tp'), may hold values from -6 to 6
- out_cotangent: bfloat16 [16384, 2048], P('fs'), may hold values from -0.046875 to 0.046875
- query_basis: bfloat16 [2048, 256], replicated, may hold values from -0.125 to 0.125
- forget_basis: bfloat16 [2048, 256], replicated, may hold values from -0.125 to 0.125
- out_basis: bfloat16 [2048, 256], replicated, may hold values from -0.125 to 0.125
- query_weight: float32 [2048, 2048], P('fs', 'tp'), may hold values from -0.125 to 0.125
- forget_weight: float32 [2048, 2048], P('fs', 'tp'), may hold values from -0.125 to 0.125
- out_weight: float32 [2048, 2048], P('fs', 'tp'), may hold values from -0.125 to 0.125
- query_first: float32 [256, 2048], P('fs', 'tp'), may hold values from -25 to 25
- forget_first: float32 [256, 2048], P('fs', 'tp'), may hold values from -25 to 25
- out_first: float32 [256, 2048], P('fs', 'tp'), may hold values from -25 to 25
- query_second: float32 [256, 2048], P('fs', 'tp'), may hold values from 0.2 to 2
- forget_second: float32 [256, 2048], P('fs', 'tp'), may hold values from 0.2 to 2
- out_second: float32 [256, 2048], P('fs', 'tp'), may hold values from 0.2 to 2
Outputs:
- query_update: float32 [2048, 2048], P('fs', 'tp')
- forget_update: float32 [2048, 2048], P('fs', 'tp')
- out_update: float32 [2048, 2048], P('fs', 'tp')
- query_first_new: float32 [256, 2048], P('fs', 'tp')
- forget_first_new: float32 [256, 2048], P('fs', 'tp')
- out_first_new: float32 [256, 2048], P('fs', 'tp')
- query_second_new: float32 [256, 2048], P('fs', 'tp')
- forget_second_new: float32 [256, 2048], P('fs', 'tp')
- out_second_new: float32 [256, 2048], P('fs', 'tp')
- query_copy: bfloat16 [2048, 2048], P(None, 'tp')
- forget_copy: bfloat16 [2048, 2048], P(None, 'tp')
- out_copy: bfloat16 [2048, 2048], P(None, 'tp')
All inputs are finite; a program needn't handle non-finite values.
Results may differ from a plain program's by a relative error of at most 0.0065.
Values may be sent and summed in bfloat16 or wider, within the bound.
A program may use at most 128 MiB of HBM per device.

v0:
```python
import jax
import jax.numpy as jnp
from jax import lax
from jax.sharding import PartitionSpec as P

WIDTH = 2048
RANK = 256
highest = lax.Precision.HIGHEST


def contract_rows(left, right):
    return lax.dot_general(
        left, right, (((0,), (0,)), ((), ())), precision=None, preferred_element_type=jnp.float32
    )


def moments(source, cotangent, basis, weight, first, second):
    row_count = weight.shape[0]
    basis_rows = lax.dynamic_slice_in_dim(
        basis, lax.axis_index("fs") * row_count, row_count, 0
    ).astype(jnp.float32)
    reduced = jnp.dot(source, basis, preferred_element_type=jnp.float32)
    reduced_high = reduced.astype(jnp.bfloat16)
    reduced_low = (reduced - reduced_high.astype(jnp.float32)).astype(jnp.bfloat16)
    projected = lax.psum_scatter(
        (contract_rows(reduced_high, cotangent) + contract_rows(reduced_low, cotangent)).astype(
            jnp.bfloat16
        ),
        "fs",
        scatter_dimension=0,
        tiled=True,
    ).astype(jnp.float32)
    first_new = 0.8 * first + 0.2 * projected
    second_new = 0.95 * second + 0.05 * projected * projected
    direction = first_new / (jnp.sqrt(second_new) + 1e-08)
    return (direction, first_new, second_new, jnp.sum(direction * direction), basis_rows)


def expand(direction, basis_rows, total, weight):
    stepped = jnp.dot(
        basis_rows, lax.all_gather(direction, "fs", axis=0, tiled=True), precision=highest
    )
    update = stepped * lax.rsqrt(total / (RANK * WIDTH) + 1e-06)
    return (update, (weight - 0.05 * update).astype(jnp.bfloat16))


def local(
    saved_input,
    query_cotangent,
    forget_cotangent,
    mixed_output,
    out_cotangent,
    query_basis,
    forget_basis,
    out_basis,
    query_weight,
    forget_weight,
    out_weight,
    query_first,
    forget_first,
    out_first,
    query_second,
    forget_second,
    out_second,
):
    query_dir, query_one, query_two, query_sq, query_rows = moments(
        saved_input, query_cotangent, query_basis, query_weight, query_first, query_second
    )
    forget_dir, forget_one, forget_two, forget_sq, forget_rows = moments(
        saved_input, forget_cotangent, forget_basis, forget_weight, forget_first, forget_second
    )
    out_dir, out_one, out_two, out_sq, out_rows = moments(
        out_cotangent, mixed_output, out_basis, out_weight, out_first, out_second
    )
    totals = lax.psum((query_sq, forget_sq, out_sq), ("fs", "tp"))
    query_step, query_new = expand(query_dir, query_rows, totals[0], query_weight)
    forget_step, forget_new = expand(forget_dir, forget_rows, totals[1], forget_weight)
    out_step, out_new = expand(out_dir, out_rows, totals[2], out_weight)
    query_copy, forget_copy, out_copy = (
        lax.all_gather(query_new, "fs", axis=0, tiled=True),
        lax.all_gather(forget_new, "fs", axis=0, tiled=True),
        lax.all_gather(out_new, "fs", axis=0, tiled=True),
    )
    return (
        query_step,
        forget_step,
        out_step,
        query_one,
        forget_one,
        out_one,
        query_two,
        forget_two,
        out_two,
        query_copy,
        forget_copy,
        out_copy,
    )


def solution(mesh):
    in_specs = (
        P("fs", None),
        P("fs", "tp"),
        P("fs", "tp"),
        P("fs", "tp"),
        P("fs", None),
        P(),
        P(),
        P(),
        P("fs", "tp"),
        P("fs", "tp"),
        P("fs", "tp"),
        P("fs", "tp"),
        P("fs", "tp"),
        P("fs", "tp"),
        P("fs", "tp"),
        P("fs", "tp"),
        P("fs", "tp"),
    )
    out_specs = (
        P("fs", "tp"),
        P("fs", "tp"),
        P("fs", "tp"),
        P("fs", "tp"),
        P("fs", "tp"),
        P("fs", "tp"),
        P("fs", "tp"),
        P("fs", "tp"),
        P("fs", "tp"),
        P(None, "tp"),
        P(None, "tp"),
        P(None, "tp"),
    )
    return jax.shard_map(local, mesh=mesh, in_specs=in_specs, out_specs=out_specs, check_vma=False)
```

profile of v0, /device:TPU:0, one launch (start us, length us, event | category | flops | bytes accessed | tf_op | source)
XLA Modules:
  0.0 426.3 jit_solution(11486083367784151921)
XLA Ops:
  7.2 6.2 %fusion.31 = f32[2048,256]{1,0:T(8,128)S(1)} fusion(bf16[2048,2048]{1,0:T(8,128)(2,1)} %param.17, bf16[2048,256]{1,0:T(8,128)(2,1)} %param.23), kind=kOutput, calls=%fused_computation.49 | convolution fusion | flops 2147483648 | bytes 11534336 | tf_op jit(solution)/shard_map/dot_general | solution.py:22
  13.5 0.8 fusion.7
  14.3 1.5 fusion.1
  15.9 6.0 %fusion.32 = f32[2048,256]{1,0:T(8,128)S(1)} fusion(bf16[2048,2048]{1,0:T(8,128)(2,1)} %param.21, bf16[2048,256]{1,0:T(8,128)(2,1)S(1)} %copy-done.13), kind=kOutput, calls=%fused_computation.50 | convolution fusion | flops 2147483648 | bytes 11534336 | tf_op jit(solution)/shard_map/dot_general | solution.py:22
  21.9 0.7 fusion.4
  22.6 1.4 fusion.2
  24.1 0.0 reduce-scatter.4.cloned.1.call-start
  24.2 6.0 %fusion.30 = f32[2048,256]{1,0:T(8,128)S(1)} fusion(bf16[2048,2048]{1,0:T(8,128)(2,1)} %param.17, bf16[2048,256]{1,0:T(8,128)(2,1)S(1)} %copy-done.14), kind=kOutput, calls=%fused_computation.48 | convolution fusion | flops 2147483648 | bytes 11534336 | tf_op jit(solution)/shard_map/dot_general | solution.py:22
  30.2 0.7 fusion.10
  31.1 1.5 fusion
  32.5 0.0 all-gather.6.cloned.1.call-start
  32.6 48.1 %reduce-scatter.6.cloned.1.call-done = bf16[32,512]{1,0:T(8,128)(2,1)} async-done(((bf16[256,512]{1,0:T(8,128)(2,1)}), bf16[32,512]{1,0:T(8,128)(2,1)}) %reduce-scatter.6.cloned.1.call-update) | async-done | bytes 32784 | tf_op jit(solution)/shard_map/reduce_scatter | solution.py:25
  80.8 2.0 multiply_reduce_fusion.1
  82.8 31.7 %all_gather.19 = f32[256,512]{1,0:T(8,128)S(1)} all-gather(f32[32,512]{1,0:T(8,128)S(1)} %get-tuple-element.20), channel_id=1, replica_groups=mesh['fs'=8,'tp'=4] {'fs'}, dimensions={0}, use_global_device_ids=true | all-gather | bytes 589824 | tf_op jit(solution)/shard_map/all_gather | solution.py:41
  114.5 31.3 %reduce-scatter.8.cloned.1.call-done = bf16[32,512]{1,0:T(8,128)(2,1)} async-done(((bf16[256,512]{1,0:T(8,128)(2,1)}), bf16[32,512]{1,0:T(8,128)(2,1)}) %reduce-scatter.8.cloned.1.call-update) | async-done | bytes 32784 | tf_op jit(solution)/shard_map/reduce_scatter | solution.py:25
  145.8 2.0 multiply_reduce_fusion
  147.9 63.0 %reduce-scatter.4.cloned.1.call-done = bf16[32,512]{1,0:T(8,128)(2,1)} async-done(((bf16[256,512]{1,0:T(8,128)(2,1)}), bf16[32,512]{1,0:T(8,128)(2,1)}) %reduce-scatter.4.cloned.1.call-update) | async-done | bytes 32784 | tf_op jit(solution)/shard_map/reduce_scatter | solution.py:25
  210.9 2.0 multiply_reduce_fusion.2
  212.9 40.4 %all-reduce = (f32[]{:T(128)}, f32[]{:T(128)}, f32[]{:T(128)}) all-reduce(f32[]{:T(128)} %get-tuple-element.23, f32[]{:T(128)} %get-tuple-element.19, f32[]{:T(128)} %get-tuple-element.15), channel_id=1, replica_groups=mesh['fs'=8,'tp'=4] {'fs','tp'}, use_global_device_ids=true, to_apply=%region_2.0 | all-reduce | flops 3 | bytes 24 | tf_op jit(solution)/shard_map/psum | solution.py:75
  254.0 2.3 subtract_convert_fusion.7
  256.3 0.0 all-gather.8.cloned.1.call-start
  257.1 32.5 %all_gather.20 = f32[256,512]{1,0:T(8,128)S(1)} all-gather(f32[32,512]{1,0:T(8,128)S(1)} %get-tuple-element.16), channel_id=1, replica_groups=mesh['fs'=8,'tp'=4] {'fs'}, dimensions={0}, use_global_device_ids=true | all-gather | bytes 589824 | tf_op jit(solution)/shard_map/all_gather | solution.py:41
  289.6 2.5 subtract_convert_fusion.6
  292.1 0.0 all-gather.4.cloned.1.call-start
  292.8 32.1 %all_gather.18 = f32[256,512]{1,0:T(8,128)S(1)} all-gather(f32[32,512]{1,0:T(8,128)S(1)} %get-tuple-element.24), channel_id=1, replica_groups=mesh['fs'=8,'tp'=4] {'fs'}, dimensions={0}, use_global_device_ids=true | all-gather | bytes 589824 | tf_op jit(solution)/shard_map/all_gather | solution.py:41
  324.9 2.3 subtract_convert_fusion.8
  327.2 35.1 %all-gather.8.cloned.1.call-done = bf16[2048,512]{1,0:T(8,128)(2,1)} async-done(((bf16[256,512]{1,0:T(8,128)(2,1)}), bf16[2048,512]{1,0:T(8,128)(2,1)}) %all-gather.8.cloned.1.call-update) | async-done | bytes 2097168 | tf_op jit(solution)/shard_map/all_gather | solution.py:82
  362.4 50.2 %all-gather.4.cloned.1.call-done = bf16[2048,512]{1,0:T(8,128)(2,1)} async-done(((bf16[256,512]{1,0:T(8,128)(2,1)}), bf16[2048,512]{1,0:T(8,128)(2,1)}) %all-gather.4.cloned.1.call-update) | async-done | bytes 2097168 | tf_op jit(solution)/shard_map/all_gather | solution.py:80
  412.6 3.2 copy.32
  415.8 1.3 copy.33
  417.1 1.0 copy-done.4
  418.1 1.3 copy.34
  (38 shorter events, 0.3 us)
Async XLA Ops:
  7.2 6.3 %copy-start = (bf16[2048,512]{1,0:T(8,128)(2,1)S(1)}, bf16[2048,512]{1,0:T(8,128)(2,1)}, u32[]{:S(2)}) copy-start(bf16[2048,512]{1,0:T(8,128)(2,1)} %param.19) | copy-start | bytes 6291460
  7.2 73.6 %reduce-scatter.6.cloned.1.call-start = ((), (), s32[]{:S(2)}) async-start(), calls=%async_computation.4 | async-start | bytes 294912 | tf_op jit(solution)/shard_map/reduce_scatter | solution.py:25
  14.3 1.6 copy-start.13
  15.8 130.0 %reduce-scatter.8.cloned.1.call-start = ((), (), s32[]{:S(2)}) async-start(), calls=%async_computation.5 | async-start | bytes 294912 | tf_op jit(solution)/shard_map/reduce_scatter | solution.py:25
  15.8 6.0 %copy-start.1 = (bf16[2048,512]{1,0:T(8,128)(2,1)S(1)}, bf16[2048,512]{1,0:T(8,128)(2,1)}, u32[]{:S(2)}) copy-start(bf16[2048,512]{1,0:T(8,128)(2,1)} %param.20) | copy-start | bytes 6291460
  22.6 1.5 copy-start.14
  24.1 186.8 %reduce-scatter.4.cloned.1.call-start = ((), (), s32[]{:S(2)}) async-start(), calls=%async_computation.3 | async-start | bytes 294912 | tf_op jit(solution)/shard_map/reduce_scatter | solution.py:25
  24.2 6.1 %copy-start.2 = (bf16[2048,512]{1,0:T(8,128)(2,1)S(1)}, bf16[2048,512]{1,0:T(8,128)(2,1)}, u32[]{:S(2)}) copy-start(bf16[2048,512]{1,0:T(8,128)(2,1)} %param.18) | copy-start | bytes 6291460
  31.0 49.8 %copy-start.7 = (f32[32,512]{1,0:T(8,128)S(1)}, f32[32,512]{1,0:T(8,128)}, u32[]{:S(2)}) copy-start(f32[32,512]{1,0:T(8,128)} %param.32) | copy-start | bytes 196612
  31.0 49.8 %copy-start.8 = (f32[32,512]{1,0:T(8,128)S(1)}, f32[32,512]{1,0:T(8,128)}, u32[]{:S(2)}) copy-start(f32[32,512]{1,0:T(8,128)} %param.29) | copy-start | bytes 196612
  31.0 114.8 %copy-start.9 = (f32[32,512]{1,0:T(8,128)S(1)}, f32[32,512]{1,0:T(8,128)}, u32[]{:S(2)}) copy-start(f32[32,512]{1,0:T(8,128)} %param.33) | copy-start | bytes 196612
  31.0 114.8 %copy-start.10 = (f32[32,512]{1,0:T(8,128)S(1)}, f32[32,512]{1,0:T(8,128)}, u32[]{:S(2)}) copy-start(f32[32,512]{1,0:T(8,128)} %param.30) | copy-start | bytes 196612
  31.0 179.8 %copy-start.11 = (f32[32,512]{1,0:T(8,128)S(1)}, f32[32,512]{1,0:T(8,128)}, u32[]{:S(2)}) copy-start(f32[32,512]{1,0:T(8,128)} %param.31) | copy-start | bytes 196612
  31.1 179.8 %copy-start.12 = (f32[32,512]{1,0:T(8,128)S(1)}, f32[32,512]{1,0:T(8,128)}, u32[]{:S(2)}) copy-start(f32[32,512]{1,0:T(8,128)} %param.28) | copy-start | bytes 196612
  32.5 221.5 %copy-start.5 = (f32[256,512]{1,0:T(8,128)S(1)}, f32[256,512]{1,0:T(8,128)}, u32[]{:S(2)}) copy-start(f32[256,512]{1,0:T(8,128)} %param.26) | copy-start | bytes 1572868
  32.5 294.7 %all-gather.6.cloned.1.call-start = ((), (), s32[]{:S(2)}) async-start(), calls=%async_computation.7 | async-start | bytes 2359296 | tf_op jit(solution)/shard_map/all_gather | solution.py:81
  256.3 68.7 %copy-start.6 = (f32[256,512]{1,0:T(8,128)S(1)}, f32[256,512]{1,0:T(8,128)}, u32[]{:S(2)}) copy-start(f32[256,512]{1,0:T(8,128)} %param.25) | copy-start | bytes 1572868
  256.3 106.1 %all-gather.8.cloned.1.call-start = ((), (), s32[]{:S(2)}) async-start(), calls=%async_computation.8 | async-start | bytes 2359296 | tf_op jit(solution)/shard_map/all_gather | solution.py:82
  292.1 120.5 %all-gather.4.cloned.1.call-start = ((), (), s32[]{:S(2)}) async-start(), calls=%async_computation.6 | async-start | bytes 2359296 | tf_op jit(solution)/shard_map/all_gather | solution.py:80
  412.6 3.2 copy-start.3
  415.8 2.3 copy-start.4
Sparse Core Ops, SparseCore 0:
  15.9 64.7 reduce-scatter.5
  84.6 61.1 reduce-scatter.7
  149.7 61.1 reduce-scatter.3
  256.4 54.7 all-gather.5
  313.8 48.5 all-gather.7
  364.9 47.6 all-gather.3
where the time goes:
time: 427 us; the launch traced here: 426 us
  waiting for transfers between devices  228 us (53%)
  blocking collectives  137 us (32%)
  matrix products  31.9 us (7%)
  between operations  16.4 us (4%)
  local copies, waits for them, and re-layouts  6.94 us (2%)
  other arithmetic  6.12 us (1%)
    reduce_scatter x3, waiting for transfers between devices, moments(): lax.psum_scatter((contract_rows(reduced_high, cotangent) + contract_rows(...  142 us
    all_gather x3, blocking collectives, expand(): lax.all_gather(direction, 'fs', axis=0, tiled=True)  96.4 us
    all_gather x1, waiting for transfers between devices, local(): lax.all_gather(query_new, 'fs', axis=0, tiled=True)  50.2 us
    psum x1, blocking collectives, local(): totals = lax.psum((query_sq, forget_sq, out_sq), ('fs', 'tp'))  40.4 us
    all_gather x1, waiting for transfers between devices, local(): lax.all_gather(out_new, 'fs', axis=0, tiled=True)  35.1 us
    dot_general x3, matrix products, moments(): reduced = jnp.dot(source, basis, preferred_element_type=jnp.float32)  18.3 us
  transfers between devices with their start and end apart: 6, of which 5 were waited for; matrix products, arithmetic and copies ran while one was open for 6% of the time, Pallas kernels for 0%

commit v1 on v0

--- a/solution.py
+++ b/solution.py
@@ -72,7 +72,9 @@
     out_dir, out_one, out_two, out_sq, out_rows = moments(
         out_cotangent, mixed_output, out_basis, out_weight, out_first, out_second
     )
-    totals = lax.psum((query_sq, forget_sq, out_sq), ("fs", "tp"))
+    totals = (query_sq, forget_sq, out_sq)
+    for idx in ("tp", "fs"):
+        totals = jax.lax.psum(totals, idx)
     query_step, query_new = expand(query_dir, query_rows, totals[0], query_weight)
     forget_step, forget_new = expand(forget_dir, forget_rows, totals[1], forget_weight)
     out_step, out_new = expand(out_dir, out_rows, totals[2], out_weight)

time: 427 us -> 412 us (0.965)
  blocking collectives: 137 us -> 123 us
    psum x1 -> x2, blocking collectives: 40.4 us -> 26.3 us  [local(): totals = jax.lax.psum(totals, idx)]
where the time goes in v1:
time: 412 us
  waiting for transfers between devices  227 us (55%)
  blocking collectives  123 us (30%)
  matrix products  31.9 us (8%)
  between operations  16.4 us (4%)
  local copies, waits for them, and re-layouts  6.94 us (2%)
  other arithmetic  6.12 us (1%)
    reduce_scatter x3, waiting for transfers between devices, moments(): lax.psum_scatter((contract_rows(reduced_high, cotangent) + contract_rows(...  142 us
    all_gather x3, blocking collectives, expand(): lax.all_gather(direction, 'fs', axis=0, tiled=True)  96.5 us
    all_gather x1, waiting for transfers between devices, local(): lax.all_gather(query_new, 'fs', axis=0, tiled=True)  50.2 us
    all_gather x1, waiting for transfers between devices, local(): lax.all_gather(out_new, 'fs', axis=0, tiled=True)  34.7 us
    psum x2, blocking collectives, local(): totals = jax.lax.psum(totals, idx)  26.3 us
    dot_general x3, matrix products, moments(): reduced = jnp.dot(source, basis, preferred_element_type=jnp.float32)  18.3 us
  transfers between devices with their start and end apart: 6, of which 5 were waited for; matrix products, arithmetic and copies ran while one was open for 6% of the time, Pallas kernels for 0%

profile of v1, /device:TPU:0, one launch (start us, length us, event | category | flops | bytes accessed | tf_op | source)
XLA Modules:
  0.0 411.9 jit_solution(6063637765545253595)
XLA Ops:
  7.2 6.2 %fusion.31 = f32[2048,256]{1,0:T(8,128)S(1)} fusion(bf16[2048,2048]{1,0:T(8,128)(2,1)} %param.17, bf16[2048,256]{1,0:T(8,128)(2,1)} %param.23), kind=kOutput, calls=%fused_computation.49 | convolution fusion | flops 2147483648 | bytes 11534336 | tf_op jit(solution)/shard_map/dot_general | solution.py:22
  13.5 0.8 fusion.7
  14.3 1.5 fusion.1
  15.9 6.0 %fusion.32 = f32[2048,256]{1,0:T(8,128)S(1)} fusion(bf16[2048,2048]{1,0:T(8,128)(2,1)} %param.21, bf16[2048,256]{1,0:T(8,128)(2,1)S(1)} %copy-done.13), kind=kOutput, calls=%fused_computation.50 | convolution fusion | flops 2147483648 | bytes 11534336 | tf_op jit(solution)/shard_map/dot_general | solution.py:22
  21.9 0.7 fusion.4
  22.6 1.4 fusion.2
  24.1 0.0 reduce-scatter.4.cloned.1.call-start
  24.2 6.0 %fusion.30 = f32[2048,256]{1,0:T(8,128)S(1)} fusion(bf16[2048,2048]{1,0:T(8,128)(2,1)} %param.17, bf16[2048,256]{1,0:T(8,128)(2,1)S(1)} %copy-done.14), kind=kOutput, calls=%fused_computation.48 | convolution fusion | flops 2147483648 | bytes 11534336 | tf_op jit(solution)/shard_map/dot_general | solution.py:22
  30.2 0.7 fusion.10
  31.1 1.5 fusion
  32.5 0.0 all-gather.6.cloned.1.call-start
  32.6 48.1 %reduce-scatter.6.cloned.1.call-done = bf16[32,512]{1,0:T(8,128)(2,1)} async-done(((bf16[256,512]{1,0:T(8,128)(2,1)}), bf16[32,512]{1,0:T(8,128)(2,1)}) %reduce-scatter.6.cloned.1.call-update) | async-done | bytes 32784 | tf_op jit(solution)/shard_map/reduce_scatter | solution.py:25
  80.8 2.0 multiply_reduce_fusion.1
  82.8 31.7 %all_gather.19 = f32[256,512]{1,0:T(8,128)S(1)} all-gather(f32[32,512]{1,0:T(8,128)S(1)} %get-tuple-element.23), channel_id=1, replica_groups=mesh['fs'=8,'tp'=4] {'fs'}, dimensions={0}, use_global_device_ids=true | all-gather | bytes 589824 | tf_op jit(solution)/shard_map/all_gather | solution.py:41
  114.5 31.3 %reduce-scatter.8.cloned.1.call-done = bf16[32,512]{1,0:T(8,128)(2,1)} async-done(((bf16[256,512]{1,0:T(8,128)(2,1)}), bf16[32,512]{1,0:T(8,128)(2,1)}) %reduce-scatter.8.cloned.1.call-update) | async-done | bytes 32784 | tf_op jit(solution)/shard_map/reduce_scatter | solution.py:25
  145.8 2.0 multiply_reduce_fusion
  147.9 63.0 %reduce-scatter.4.cloned.1.call-done = bf16[32,512]{1,0:T(8,128)(2,1)} async-done(((bf16[256,512]{1,0:T(8,128)(2,1)}), bf16[32,512]{1,0:T(8,128)(2,1)}) %reduce-scatter.4.cloned.1.call-update) | async-done | bytes 32784 | tf_op jit(solution)/shard_map/reduce_scatter | solution.py:25
  210.9 2.0 multiply_reduce_fusion.2
  212.9 6.3 %all-reduce.1 = (f32[]{:T(128)}, f32[]{:T(128)}, f32[]{:T(128)}) all-reduce(f32[]{:T(128)} %get-tuple-element.26, f32[]{:T(128)} %get-tuple-element.22, f32[]{:T(128)} %get-tuple-element.18), channel_id=1, replica_groups=mesh['fs'=8,'tp'=4] {'tp'}, use_global_device_ids=true, to_apply=%region_2.0 | all-reduce | flops 3 | bytes 24 | tf_op jit(solution)/shard_map/psum | solution.py:77
  219.2 20.1 %all-reduce = (f32[]{:T(128)}, f32[]{:T(128)}, f32[]{:T(128)}) all-reduce(f32[]{:T(128)} %get-tuple-element.15, f32[]{:T(128)} %get-tuple-element.16, f32[]{:T(128)} %get-tuple-element.17), channel_id=1, replica_groups=mesh['fs'=8,'tp'=4] {'fs'}, use_global_device_ids=true, to_apply=%region_3.0 | all-reduce | flops 3 | bytes 24 | tf_op jit(solution)/shard_map/psum | solution.py:77
  240.0 2.3 subtract_convert_fusion.7
  243.0 32.4 %all_gather.20 = f32[256,512]{1,0:T(8,128)S(1)} all-gather(f32[32,512]{1,0:T(8,128)S(1)} %get-tuple-element.19), channel_id=1, replica_groups=mesh['fs'=8,'tp'=4] {'fs'}, dimensions={0}, use_global_device_ids=true | all-gather | bytes 589824 | tf_op jit(solution)/shard_map/all_gather | solution.py:41
  275.5 2.5 subtract_convert_fusion.6
  278.0 0.0 all-gather.4.cloned.1.call-start
  278.7 32.3 %all_gather.18 = f32[256,512]{1,0:T(8,128)S(1)} all-gather(f32[32,512]{1,0:T(8,128)S(1)} %get-tuple-element.27), channel_id=1, replica_groups=mesh['fs'=8,'tp'=4] {'fs'}, dimensions={0}, use_global_device_ids=true | all-gather | bytes 589824 | tf_op jit(solution)/shard_map/all_gather | solution.py:41
  311.0 2.3 subtract_convert_fusion.8
  313.3 34.7 %all-gather.8.cloned.1.call-done = bf16[2048,512]{1,0:T(8,128)(2,1)} async-done(((bf16[256,512]{1,0:T(8,128)(2,1)}), bf16[2048,512]{1,0:T(8,128)(2,1)}) %all-gather.8.cloned.1.call-update) | async-done | bytes 2097168 | tf_op jit(solution)/shard_map/all_gather | solution.py:84
  348.0 50.2 %all-gather.4.cloned.1.call-done = bf16[2048,512]{1,0:T(8,128)(2,1)} async-done(((bf16[256,512]{1,0:T(8,128)(2,1)}), bf16[2048,512]{1,0:T(8,128)(2,1)}) %all-gather.4.cloned.1.call-update) | async-done | bytes 2097168 | tf_op jit(solution)/shard_map/all_gather | solution.py:82
  398.2 3.2 copy.32
  401.4 1.3 copy.33
  402.7 1.0 copy-done.4
  403.8 1.3 copy.34
  (39 shorter events, 0.3 us)
Async XLA Ops:
  7.2 6.3 %copy-start = (bf16[2048,512]{1,0:T(8,128)(2,1)S(1)}, bf16[2048,512]{1,0:T(8,128)(2,1)}, u32[]{:S(2)}) copy-start(bf16[2048,512]{1,0:T(8,128)(2,1)} %param.19) | copy-start | bytes 6291460
  7.2 73.6 %reduce-scatter.6.cloned.1.call-start = ((), (), s32[]{:S(2)}) async-start(), calls=%async_computation.4 | async-start | bytes 294912 | tf_op jit(solution)/shard_map/reduce_scatter | solution.py:25
  14.3 1.6 copy-start.13
  15.8 130.0 %reduce-scatter.8.cloned.1.call-start = ((), (), s32[]{:S(2)}) async-start(), calls=%async_computation.5 | async-start | bytes 294912 | tf_op jit(solution)/shard_map/reduce_scatter | solution.py:25
  15.8 6.0 %copy-start.1 = (bf16[2048,512]{1,0:T(8,128)(2,1)S(1)}, bf16[2048,512]{1,0:T(8,128)(2,1)}, u32[]{:S(2)}) copy-start(bf16[2048,512]{1,0:T(8,128)(2,1)} %param.20) | copy-start | bytes 6291460
  22.6 1.5 copy-start.14
  24.1 186.8 %reduce-scatter.4.cloned.1.call-start = ((), (), s32[]{:S(2)}) async-start(), calls=%async_computation.3 | async-start | bytes 294912 | tf_op jit(solution)/shard_map/reduce_scatter | solution.py:25
  24.2 6.1 %copy-start.2 = (bf16[2048,512]{1,0:T(8,128)(2,1)S(1)}, bf16[2048,512]{1,0:T(8,128)(2,1)}, u32[]{:S(2)}) copy-start(bf16[2048,512]{1,0:T(8,128)(2,1)} %param.18) | copy-start | bytes 6291460
  31.0 49.8 %copy-start.7 = (f32[32,512]{1,0:T(8,128)S(1)}, f32[32,512]{1,0:T(8,128)}, u32[]{:S(2)}) copy-start(f32[32,512]{1,0:T(8,128)} %param.32) | copy-start | bytes 196612
  31.0 49.8 %copy-start.8 = (f32[32,512]{1,0:T(8,128)S(1)}, f32[32,512]{1,0:T(8,128)}, u32[]{:S(2)}) copy-start(f32[32,512]{1,0:T(8,128)} %param.29) | copy-start | bytes 196612
  31.0 114.8 %copy-start.9 = (f32[32,512]{1,0:T(8,128)S(1)}, f32[32,512]{1,0:T(8,128)}, u32[]{:S(2)}) copy-start(f32[32,512]{1,0:T(8,128)} %param.33) | copy-start | bytes 196612
  31.0 114.8 %copy-start.10 = (f32[32,512]{1,0:T(8,128)S(1)}, f32[32,512]{1,0:T(8,128)}, u32[]{:S(2)}) copy-start(f32[32,512]{1,0:T(8,128)} %param.30) | copy-start | bytes 196612
  31.0 179.8 %copy-start.11 = (f32[32,512]{1,0:T(8,128)S(1)}, f32[32,512]{1,0:T(8,128)}, u32[]{:S(2)}) copy-start(f32[32,512]{1,0:T(8,128)} %param.31) | copy-start | bytes 196612
  31.1 179.8 %copy-start.12 = (f32[32,512]{1,0:T(8,128)S(1)}, f32[32,512]{1,0:T(8,128)}, u32[]{:S(2)}) copy-start(f32[32,512]{1,0:T(8,128)} %param.28) | copy-start | bytes 196612
  32.5 207.4 %copy-start.5 = (f32[256,512]{1,0:T(8,128)S(1)}, f32[256,512]{1,0:T(8,128)}, u32[]{:S(2)}) copy-start(f32[256,512]{1,0:T(8,128)} %param.26) | copy-start | bytes 1572868
  32.5 280.8 %all-gather.6.cloned.1.call-start = ((), (), s32[]{:S(2)}) async-start(), calls=%async_computation.7 | async-start | bytes 2359296 | tf_op jit(solution)/shard_map/all_gather | solution.py:83
  242.2 68.8 %copy-start.6 = (f32[256,512]{1,0:T(8,128)S(1)}, f32[256,512]{1,0:T(8,128)}, u32[]{:S(2)}) copy-start(f32[256,512]{1,0:T(8,128)} %param.25) | copy-start | bytes 1572868
  242.3 105.8 %all-gather.8.cloned.1.call-start = ((), (), s32[]{:S(2)}) async-start(), calls=%async_computation.8 | async-start | bytes 2359296 | tf_op jit(solution)/shard_map/all_gather | solution.py:84
  278.0 120.3 %all-gather.4.cloned.1.call-start = ((), (), s32[]{:S(2)}) async-start(), calls=%async_computation.6 | async-start | bytes 2359296 | tf_op jit(solution)/shard_map/all_gather | solution.py:82
  398.2 3.2 copy-start.3
  401.4 2.3 copy-start.4
Sparse Core Ops, SparseCore 0:
  15.9 64.7 reduce-scatter.5
  84.6 61.1 reduce-scatter.7
  149.7 61.1 reduce-scatter.3
  242.4 54.5 all-gather.5
  299.6 48.4 all-gather.7
  350.6 47.6 all-gather.3
